TPU v7x, 32 devices: a whole 2x2x4 slice. The times are simulated.
32 devices in a mesh: rep: 2 (over y), fs: 4 (over z), tp: 4 (over x, core).
Axes of the slice: x: 2, y: 2, z: 4, core: 2. Of those that a mesh axis runs over, the one named last changes fastest.
Arguments:
- tokens: bfloat16 [4096, 2048], P(('rep', 'fs')), may hold values from -6 to 6
- norm_gain: float32 [2048], replicated, may hold values from 0.1 to 1.9
- up_weight: bfloat16 [2048, 4096], P('fs', 'tp'), may hold values from -0.125 to 0.125
- down_weight: bfloat16 [4096, 2048], P('tp', 'fs'), may hold values from -0.09375 to 0.09375
Outputs:
- result: bfloat16 [4096, 2048], P(('rep', 'fs', 'tp'))
All inputs are finite; a program needn't handle non-finite values.
Results may differ from a plain program's by a relative error of at most 0.012.
Values may be sent and summed in bfloat16 or wider, within the bound.
A program may use at most 64 MiB of HBM per device.

v0:
```python
import jax
import jax.numpy as jnp
from jax import lax
from jax.sharding import PartitionSpec as P

EPS = 1e-06


def shards(tokens, norm_gain, up_weight, down_weight):
    xf = tokens.astype(jnp.float32)
    scale = lax.rsqrt(jnp.mean(xf * xf, axis=-1, keepdims=True) + EPS)
    normed = (xf * scale * norm_gain).astype(jnp.bfloat16)
    rows = tokens.shape[0]
    halves = lax.axis_size("rep")
    share = up_weight.shape[0] // halves
    mine = lax.dynamic_slice_in_dim(up_weight, lax.axis_index("rep") * share, share, 0)
    arranged = normed.reshape(rows, -1, halves, share).transpose(0, 2, 1, 3).reshape(rows, -1)
    lifted = jnp.dot(
        arranged,
        lax.all_gather(mine, ("rep", "fs"), axis=0, tiled=True),
        preferred_element_type=jnp.float32,
    )
    width = down_weight.shape[1] // halves
    down_mine = lax.dynamic_slice_in_dim(down_weight, lax.axis_index("rep") * width, width, 1)
    collected = lax.all_gather(down_mine, ("rep", "fs"), axis=1, tiled=True)
    hidden_rows = collected.shape[0]
    down_block = (
        collected.reshape(hidden_rows, halves, -1, width)
        .transpose(0, 2, 1, 3)
        .reshape(hidden_rows, -1)
    )
    hidden = jnp.square(jnp.maximum(lifted, 0.0)).astype(jnp.bfloat16)
    own_rows = rows // lax.axis_size("tp")
    summed = lax.psum_scatter(
        jnp.dot(hidden, down_block, preferred_element_type=jnp.float32).astype(jnp.bfloat16),
        "tp",
        scatter_dimension=0,
        tiled=True,
    ).astype(jnp.float32)
    residual = lax.dynamic_slice_in_dim(xf, lax.axis_index("tp") * own_rows, own_rows, 0)
    return (residual + summed).astype(jnp.bfloat16)


def solution(mesh):
    placed = (P(("rep", "fs"), None), P(), P("fs", "tp"), P("tp", "fs"))
    return jax.shard_map(
        shards, mesh=mesh, in_specs=placed, out_specs=P(("rep", "fs", "tp"), None), check_vma=False
    )
```

profile of v0, /device:TPU:0, one launch (start us, length us, event | category | flops | bytes accessed | tf_op | source)
XLA Modules:
  0.0 208.4 jit_solution(14472330394279281038)
XLA Ops:
  6.5 0.0 copy-start
  6.5 0.0 all-gather.5.cloned.1.call-start
  6.6 1.2 copy-done
  7.8 0.8 constant_dynamic-slice_fusion
  8.6 2.1 copy.9
  10.6 0.0 all-gather.5.cloned.1.call-update
  10.7 0.0 all-gather.3.cloned.1.call-start
  10.7 1.9 constant_dynamic-slice_fusion.1
  12.6 0.0 all-gather.3.cloned.1.call-update
  12.6 0.0 reduce-scatter.2.cloned.1.call-start
  12.7 0.0 copy-done.1
  12.7 0.5 multiply_reduce_fusion
  13.2 0.0 copy-done.2
  13.2 1.9 multiply_convert_fusion
  15.1 4.5 %reshape.21 = bf16[512,4,2,256]{3,2,1,0:T(2,128)(2,1)} reshape(bf16[512,2048]{1,0:T(8,128)(2,1)} %multiply_convert_fusion) | data formatting | bytes 4194304 | tf_op jit(solution)/shard_map/reshape | solution.py:17
  19.6 6.2 %copy.6 = bf16[512,4,2,256]{0,3,1,2:T(8,128)(2,1)} copy(bf16[512,4,2,256]{3,2,1,0:T(2,128)(2,1)} %reshape.21) | data formatting | bytes 4194304 | tf_op jit(solution)/shard_map/reshape | solution.py:17
  25.7 60.6 %all-gather.5.cloned.1.call-done = bf16[1024,2048]{0,1:T(8,128)(2,1)} async-done(((bf16[1024,256]{0,1:T(8,128)(2,1)}), bf16[1024,2048]{0,1:T(8,128)(2,1)}) %all-gather.5.cloned.1.call-update) | async-done | bytes 4194320 | tf_op jit(solution)/shard_map/all_gather | solution.py:25
  86.3 4.6 %copy.8 = bf16[1024,4,2,256]{0,3,2,1:T(8,128)(2,1)} copy(bf16[1024,4,2,256]{0,3,1,2:T(8,128)(2,1)} %bitcast.10) | data formatting | bytes 8388608 | tf_op jit(solution)/shard_map/transpose | solution.py:29
  90.9 68.9 %all-gather.3.cloned.1.call-done = bf16[2048,1024]{1,0:T(8,128)(2,1)} async-done(((bf16[256,1024]{1,0:T(8,128)(2,1)}), bf16[2048,1024]{1,0:T(8,128)(2,1)}) %all-gather.3.cloned.1.call-update) | async-done | bytes 4194320 | tf_op jit(solution)/shard_map/all_gather | solution.py:20
  159.8 9.9 %convolution_convert_fusion = bf16[512,2048]{1,0:T(8,128)(2,1)} fusion(bf16[1024,2048]{0,1:T(8,128)(2,1)} %bitcast.11, bf16[512,2048]{0,1:T(8,128)(2,1)} %bitcast.12, bf16[2048,1024]{1,0:T(8,128)(2,1)} %all-gather.3.cloned.1.call-done), kind=kOutput, calls=%fused_computation.2 | convolution fusion | flops 4297588736 | bytes 12582912 | tf_op jit(solution)/shard_map/dot_general | solution.py:35
  169.7 0.0 reduce-scatter.2.cloned.1.call-update
  169.8 2.5 %convert_element_type.18 = f32[512,2048]{1,0:T(8,128)} convert(bf16[512,2048]{1,0:T(8,128)(2,1)S(1)} %copy-done.1) | non-fusion elementwise | flops 1048576 | bytes 6291456 | tf_op jit(solution)/shard_map/convert_element_type | solution.py:10
  172.2 27.4 %reduce-scatter.2.cloned.1.call-done = bf16[128,2048]{1,0:T(8,128)(2,1)} async-done(((bf16[512,2048]{1,0:T(8,128)(2,1)}), bf16[128,2048]{1,0:T(8,128)(2,1)}) %reduce-scatter.2.cloned.1.call-update) | async-done | bytes 524304 | tf_op jit(solution)/shard_map/reduce_scatter | solution.py:34
  199.6 2.3 %add_convert_fusion = bf16[128,2048]{1,0:T(8,128)(2,1)} fusion(bf16[128,2048]{1,0:T(8,128)(2,1)} %reduce-scatter.2.cloned.1.call-done, f32[512,2048]{1,0:T(8,128)} %convert_element_type.18, s32[]{:T(128)S(6)} %select_n.7), kind=kLoop, calls=%fused_computation.4 | loop fusion | flops 786432 | bytes 2097156 | tf_op jit(solution)/shard_map/convert_element_type | solution.py:41
  (3 shorter events, 0.0 us)
Async XLA Ops:
  6.5 1.2 copy-start
  6.5 6.1 %copy-start.1 = (bf16[512,2048]{1,0:T(8,128)(2,1)S(1)}, bf16[512,2048]{1,0:T(8,128)(2,1)}, u32[]{:S(2)}) copy-start(bf16[512,2048]{1,0:T(8,128)(2,1)} %param.4) | copy-start | bytes 6291460
  6.5 6.6 %copy-start.2 = (f32[2048]{0:T(1024)S(1)}, f32[2048]{0:T(1024)}, u32[]{:S(2)}) copy-start(f32[2048]{0:T(1024)} %param.5) | copy-start | bytes 24580
  6.5 79.8 %all-gather.5.cloned.1.call-start = ((), (), s32[]{:S(2)}) async-start(), calls=%async_computation.2 | async-start | bytes 4718592 | tf_op jit(solution)/shard_map/all_gather | solution.py:25
  10.7 149.2 %all-gather.3.cloned.1.call-start = ((), (), s32[]{:S(2)}) async-start(), calls=%async_computation.1 | async-start | bytes 4718592 | tf_op jit(solution)/shard_map/all_gather | solution.py:20
  12.6 187.0 %reduce-scatter.2.cloned.1.call-start = ((), (), s32[]{:S(2)}) async-start(), calls=%async_computation.3 | async-start | bytes 2621440 | tf_op jit(solution)/shard_map/reduce_scatter | solution.py:34
Sparse Core Ops, SparseCore 0:
  10.8 75.4 all-gather.4
  88.5 71.3 all-gather.2
  169.9 29.6 reduce-scatter.1
where the time goes:
time: 209 us; the launch traced here: 208 us
  waiting for transfers between devices  157 us (75%)
  local copies, waits for them, and re-layouts  21.2 us (10%)
  between operations  13.1 us (6%)
  matrix products  9.9 us (5%)
  other arithmetic  7.13 us (3%)
    all_gather x1, waiting for transfers between devices, shards(): lax.all_gather(mine, ('rep', 'fs'), axis=0, tiled=True)  68.9 us
    all_gather x1, waiting for transfers between devices, shards(): collected = lax.all_gather(down_mine, ('rep', 'fs'), axis=1, tiled=True)  60.6 us
    reduce_scatter x1, waiting for transfers between devices, shards(): lax.psum_scatter(jnp.dot(hidden, down_block, preferred_element_type=jnp.f...  27.4 us
    reshape x2, local copies, waits for them, and re-layouts, shards(): normed.reshape(rows, -1, halves, share).transpose(0, 2, 1, 3)  10.7 us
    dot_general x1, matrix products, shards(): jnp.dot(hidden, down_block, preferred_element_type=jnp.float32)  9.9 us
    transpose x1, local copies, waits for them, and re-layouts, shards(): down_block = collected.reshape(hidden_rows, halves, -1, width).transpose(...  4.59 us
  transfers between devices with their start and end apart: 3, of which 3 were waited for; matrix products, arithmetic and copies ran while one was open for 11% of the time, Pallas kernels for 0%

commit v1 on v0

--- a/solution.py
+++ b/solution.py
@@ -1,9 +1,15 @@
+import functools
+
 import jax
 import jax.numpy as jnp
 from jax import lax
+from jax.experimental import pallas as pl
+from jax.experimental.pallas import tpu as pltpu
 from jax.sharding import PartitionSpec as P
 
 EPS = 1e-06
+UP_CHUNKS = 2
+CHUNK_COLS = 256
 
 
 def shards(tokens, norm_gain, up_weight, down_weight):
@@ -41,8 +47,322 @@
     return (residual + summed).astype(jnp.bfloat16)
 
 
+def kernel(
+    n, tok_hbm, gain_ref, up_hbm, dn_hbm, out_hbm,
+    tok, nrm, upw, dnw, hid, acc, keep, asend, arecv, bsend, brecv, outv,
+    up_send, up_recv, dn_send, dn_recv, tok_send, tok_recv,
+    a_send, a_recv, b_send, b_recv, local, out_sem,
+):
+    y, z, t = lax.axis_index("rep"), lax.axis_index("fs"), lax.axis_index("tp")
+    x, core = t // 2, t % 2
+    partner = x * 2 + (1 - core)
+    rows = tok_hbm.shape[0]
+    own_rows = rows // 4
+    up_rows = up_hbm.shape[0]
+    H = upw.shape[1]
+    CW = dnw.shape[2]
+    DC = dn_hbm.shape[1] // CW
+    UC = UP_CHUNKS
+    piece = up_rows // UC
+    half = rows // 2
+    total = n * DC
+
+    def at(yy, zz, tt):
+        return {"rep": yy, "fs": zz, "tp": tt}
+
+    def remote(src, dst, send, recv, where):
+        return pltpu.make_async_remote_copy(
+            src_ref=src, dst_ref=dst, send_sem=send, recv_sem=recv,
+            device_id=where, device_id_type=pl.DeviceIdType.MESH,
+        )
+
+    def beside(side):
+        return at(y, z - 1 if side == 0 else z + 1, t)
+
+    def up_slot(s, c):
+        return upw.at[pl.ds(pl.multiple_of(s * up_rows + c * piece, piece), piece), :]
+
+    def up_own(c):
+        return up_hbm.at[pl.ds(c * piece, piece), pl.ds(pl.multiple_of(y * H, H), H)]
+
+    def dn_own(c):
+        return dn_hbm.at[pl.ds(pl.multiple_of(y * H, H), H), pl.ds(c * CW, CW)]
+
+    def up_copy(side, s, c, src):
+        return remote(src, up_slot(s, c), up_send.at[side, s * UC + c],
+                      up_recv.at[s * UC + c], beside(side))
+
+    def dn_copy(side, s, c, src):
+        return remote(src, dnw.at[s * DC + c], dn_send.at[side, s * DC + c],
+                      dn_recv.at[s * DC + c], beside(side))
+
+    def send_own_dn(side):
+        for c in range(DC):
+            dn_copy(side, z, c, dn_own(c)).start()
+
+    def source(p):
+        m = jnp.minimum(z, n - 1 - z)
+        k = jnp.where(p <= 2 * m, (p + 1) // 2, p - m)
+        sign = jnp.where(
+            p <= 2 * m, jnp.where(p % 2 == 1, 1, -1), jnp.where(z < n - 1 - z, 1, -1)
+        )
+        return z + sign * k
+
+    loads = [pltpu.make_async_copy(tok_hbm, tok.at[y], local.at[0])]
+    for c in range(UC):
+        loads.append(pltpu.make_async_copy(up_own(c), up_slot(z, c), local.at[1 + c]))
+    for c in range(DC):
+        loads.append(pltpu.make_async_copy(dn_own(c), dnw.at[z * DC + c], local.at[1 + UC + c]))
+    for load in loads:
+        load.start()
+
+    peers = [at(y, z, partner)]
+    for j in (1, 2, 3):
+        peers.append(at((y + j // 2) % 2, z, ((x + j % 2) % 2) * 2 + core))
+    barrier = pltpu.get_barrier_semaphore()
+    for peer in peers:
+        pl.semaphore_signal(barrier, inc=1, device_id=peer, device_id_type=pl.DeviceIdType.MESH)
+    has = (z > 0, z < n - 1)
+    for side in (0, 1):
+        @pl.when(has[side])
+        def _():
+            pl.semaphore_signal(
+                barrier, inc=1, device_id=beside(side), device_id_type=pl.DeviceIdType.MESH
+            )
+    greeted = 4 + jnp.where(has[0], 1, 0) + jnp.where(has[1], 1, 0)
+    pl.semaphore_wait(barrier, greeted)
+
+    for side in (0, 1):
+        @pl.when(has[side])
+        def _():
+            for c in range(UC):
+                up_copy(side, z, c, up_own(c)).start()
+
+    part = pl.ds(pl.multiple_of(core * half, half), half)
+    across = remote(tok_hbm.at[part, :], tok.at[y, part, :], tok_send.at[0], tok_recv.at[0],
+                    at(1 - y, z, t))
+    across.start()
+
+    @pl.when(z == 0)
+    def _():
+        send_own_dn(1)
+
+    @pl.when(z == n - 1)
+    def _():
+        send_own_dn(0)
+
+    gain = gain_ref[...]
+
+    def normalise(yy):
+        def tile(i, carry):
+            xf = tok[yy, pl.ds(pl.multiple_of(i * own_rows, own_rows), own_rows), :].astype(jnp.float32)
+            scale = lax.rsqrt(jnp.mean(xf * xf, axis=-1, keepdims=True) + EPS)
+            to = (i % 2) * rows + (yy * 2 + i // 2) * own_rows
+            nrm[pl.ds(pl.multiple_of(to, own_rows), own_rows), :] = (xf * scale * gain).astype(jnp.bfloat16)
+            return carry
+        lax.fori_loop(0, 4, tile, 0)
+
+    loads[0].wait()
+    normalise(y)
+
+    for p in range(1, n):
+        s = source(p)
+        for c in range(UC):
+            up_copy(0, s, c, up_slot(s, c)).wait_recv()
+            for side in (0, 1):
+                @pl.when(((s > z) if side == 0 else (s < z)) & has[side])
+                def _():
+                    up_copy(side, s, c, up_slot(s, c)).start()
+        for side in (0, 1):
+            @pl.when((s == (n - 1 if side == 0 else 0)) & has[side])
+            def _():
+                send_own_dn(side)
+
+    theirs = pl.ds(pl.multiple_of((1 - core) * half, half), half)
+    across.wait_recv()
+    over = remote(tok.at[1 - y, part, :], tok.at[1 - y, part, :], tok_send.at[1], tok_recv.at[1],
+                  at(y, z, partner))
+    over.start()
+    remote(tok.at[1 - y, theirs, :], tok.at[1 - y, theirs, :], tok_send.at[1], tok_recv.at[1],
+           at(y, z, partner)).wait_recv()
+    normalise(1 - y)
+    for load in loads[1:]:
+        load.wait()
+
+    def lift(i, carry):
+        r = pl.ds(pl.multiple_of(i * half, half), half)
+        lifted = jnp.dot(nrm[r, :], upw[...], preferred_element_type=jnp.float32)
+        hid[r, :] = jnp.square(jnp.maximum(lifted, 0.0)).astype(jnp.bfloat16)
+        return carry
+
+    lax.fori_loop(0, 2 * rows // half, lift, 0)
+
+    own_q = y * 2 + x
+
+    def a_copy(i):
+        return remote(asend.at[i], arecv.at[i], a_send.at[i], a_recv.at[i], at(y, z, partner))
+
+    def b_copy(i, j):
+        yy, xx = (y + j // 2) % 2, (x + j % 2) % 2
+        return remote(bsend.at[i, yy * 2 + xx], brecv.at[i, j - 1], b_send.at[i, j - 1],
+                      b_recv.at[i, j - 1], at(yy, z, xx * 2 + core))
+
+    def out_copy(i):
+        column = (source(i // DC) * DC + i % DC) * CW
+        return pltpu.make_async_copy(
+            outv.at[i], out_hbm.at[:, pl.ds(pl.multiple_of(column, CW), CW)], out_sem.at[i]
+        )
+
+    def finish(i):
+        for j in (1, 2, 3):
+            b_copy(i, j).wait_recv()
+        column = (source(i // DC) * DC + i % DC) * CW
+        res = tok[y, pl.ds(pl.multiple_of(t * own_rows, own_rows), own_rows),
+                  pl.ds(pl.multiple_of(column, CW), CW)].astype(jnp.float32)
+        res = res + keep[i]
+        for j in range(3):
+            res = res + brecv[i, j].astype(jnp.float32)
+        outv[i] = res.astype(jnp.bfloat16)
+        out_copy(i).start()
+
+    def step(i, carry):
+        p, c = i // DC, i % DC
+        s = source(p)
+
+        @pl.when(p > 0)
+        def _():
+            dn_copy(0, s, c, dnw.at[s * DC + c]).wait_recv()
+            for side in (0, 1):
+                @pl.when(((s > z) if side == 0 else (s < z)) & has[side])
+                def _():
+                    dn_copy(side, s, c, dnw.at[s * DC + c]).start()
+
+        block = dnw[s * DC + c]
+        first = hid[pl.ds(pl.multiple_of((1 - core) * rows, rows), rows), :]
+        asend[i] = jnp.dot(first, block, preferred_element_type=jnp.float32).astype(jnp.bfloat16)
+        a_copy(i).start()
+        second = hid[pl.ds(pl.multiple_of(core * rows, rows), rows), :]
+        acc[...] = jnp.dot(second, block, preferred_element_type=jnp.float32)
+        a_copy(i).wait_recv()
+        for q in range(4):
+            r = pl.ds(q * own_rows, own_rows)
+            bsend[i, q] = (acc[r, :] + arecv[i, r, :].astype(jnp.float32)).astype(jnp.bfloat16)
+        for j in (3, 2, 1):
+            b_copy(i, j).start()
+        r = pl.ds(pl.multiple_of(own_q * own_rows, own_rows), own_rows)
+        keep[i] = acc[r, :] + arecv[i, r, :].astype(jnp.float32)
+
+        @pl.when(i > 0)
+        def _():
+            finish(i - 1)
+        return carry
+
+    lax.fori_loop(0, total, step, 0)
+    finish(total - 1)
+
+    across.wait_send()
+    over.wait_send()
+
+    def drain(i, carry):
+        a_copy(i).wait_send()
+        for j in (1, 2, 3):
+            b_copy(i, j).wait_send()
+        out_copy(i).wait()
+        return carry
+
+    lax.fori_loop(0, total, drain, 0)
+    for side in (0, 1):
+        for s in range(n):
+            @pl.when(((z <= s) if side == 0 else (z >= s)) & has[side])
+            def _():
+                for c in range(UC):
+                    up_copy(side, s, c, up_slot(s, c)).wait_send()
+                for c in range(DC):
+                    dn_copy(side, s, c, dnw.at[s * DC + c]).wait_send()
+
+
+def fused(n, tokens, norm_gain, up_weight, down_weight):
+    rows, D = tokens.shape
+    up_rows, block = up_weight.shape
+    H = block // 2
+    CW = CHUNK_COLS
+    DC = down_weight.shape[1] // CW
+    total = n * DC
+    own_rows = rows // 4
+    bf, f32 = jnp.bfloat16, jnp.float32
+    dma = pltpu.SemaphoreType.DMA
+    return pl.pallas_call(
+        functools.partial(kernel, n),
+        out_shape=jax.ShapeDtypeStruct((own_rows, D), bf),
+        in_specs=[
+            pl.BlockSpec(memory_space=pl.ANY),
+            pl.BlockSpec(memory_space=pltpu.VMEM),
+            pl.BlockSpec(memory_space=pl.ANY),
+            pl.BlockSpec(memory_space=pl.ANY),
+        ],
+        out_specs=pl.BlockSpec(memory_space=pl.ANY),
+        scratch_shapes=[
+            pltpu.VMEM((2, rows, D), bf),
+            pltpu.VMEM((2 * rows, D), bf),
+            pltpu.VMEM((n * up_rows, H), bf),
+            pltpu.VMEM((n * DC, H, CW), bf),
+            pltpu.VMEM((2 * rows, H), bf),
+            pltpu.VMEM((rows, CW), f32),
+            pltpu.VMEM((total, own_rows, CW), f32),
+            pltpu.VMEM((total, rows, CW), bf),
+            pltpu.VMEM((total, rows, CW), bf),
+            pltpu.VMEM((total, 4, own_rows, CW), bf),
+            pltpu.VMEM((total, 3, own_rows, CW), bf),
+            pltpu.VMEM((total, own_rows, CW), bf),
+            dma((2, n * UP_CHUNKS)),
+            dma((n * UP_CHUNKS,)),
+            dma((2, n * DC)),
+            dma((n * DC,)),
+            dma((2,)),
+            dma((2,)),
+            dma((total,)),
+            dma((total,)),
+            dma((total, 3)),
+            dma((total, 3)),
+            dma((1 + UP_CHUNKS + DC,)),
+            dma((total,)),
+        ],
+        compiler_params=pltpu.CompilerParams(
+            collective_id=0, has_side_effects=True, vmem_limit_bytes=58 * 1024 * 1024
+        ),
+    )(tokens, norm_gain.reshape(1, D), up_weight, down_weight)
+
+
+def fits(mesh, tokens, up_weight, down_weight):
+    n = mesh.shape["fs"]
+    rows = tokens.shape[0] // (mesh.shape["rep"] * n)
+    columns = down_weight.shape[1] // n
+    depth = up_weight.shape[0] // n
+    hidden = up_weight.shape[1] // mesh.shape["tp"]
+    return (
+        mesh.shape["rep"] == 2
+        and mesh.shape["tp"] == 4
+        and n <= 8
+        and columns % CHUNK_COLS == 0
+        and depth % (UP_CHUNKS * 16) == 0
+        and hidden % 256 == 0
+        and rows % 64 == 0
+        and rows <= 512
+        and hidden <= 1024
+        and tokens.shape[1] <= 2048
+    )
+
+
 def solution(mesh):
     placed = (P(("rep", "fs"), None), P(), P("fs", "tp"), P("tp", "fs"))
-    return jax.shard_map(
-        shards, mesh=mesh, in_specs=placed, out_specs=P(("rep", "fs", "tp"), None), check_vma=False
-    )
+
+    def layer(tokens, norm_gain, up_weight, down_weight):
+        if fits(mesh, tokens, up_weight, down_weight):
+            body = functools.partial(fused, mesh.shape["fs"])
+        else:
+            body = shards
+        return jax.shard_map(
+            body, mesh=mesh, in_specs=placed, out_specs=P(("rep", "fs", "tp"), None), check_vma=False
+        )(tokens, norm_gain, up_weight, down_weight)
+
+    return layer

time: 209 us -> 83.9 us (0.40)
  waiting for transfers between devices: 157 us -> 0 us
  Pallas kernels: 0 us -> 81.4 us
  local copies, waits for them, and re-layouts: 21.2 us -> 1.88 us
  between operations: 13.1 us -> 0.01 us
  matrix products: 9.9 us -> 0 us
  other arithmetic: 7.13 us -> 0 us
    all_gather x2 -> x0, waiting for transfers between devices: 130 us -> none  [the longest x1 68.9 us: shards(): lax.all_gather(mine, ('rep', 'fs'), axis=0, tiled=True)]
    pallas_call x0 -> x1, Pallas kernels: none -> 81.4 us  [fused(): pl.pallas_call(functools.partial(kernel, n), out_shape=jax.ShapeDtypeStru...]
    reduce_scatter x1 -> x0, waiting for transfers between devices: 27.4 us -> none  [shards(): lax.psum_scatter(jnp.dot(hidden, down_block, preferred_element_type=jnp.f...]
    reshape x2 -> x0, local copies, waits for them, and re-layouts: 10.7 us -> none  [shards(): normed.reshape(rows, -1, halves, share).transpose(0, 2, 1, 3)]
    dot_general x1 -> x0, matrix products: 9.9 us -> none  [shards(): jnp.dot(hidden, down_block, preferred_element_type=jnp.float32)]
    convert_element_type x3 -> x0, other arithmetic: 6.64 us -> none  [the longest x1 2.47 us: shards(): xf = tokens.astype(jnp.float32)]
    transpose x1 -> x0, local copies, waits for them, and re-layouts: 4.59 us -> none  [shards(): down_block = collected.reshape(hidden_rows, halves, -1, width).transpose(...]
    dynamic_slice x2 -> x0, local copies, waits for them, and re-layouts: 2.7 us -> none  [the longest x1 1.88 us: shards(): lax.dynamic_slice_in_dim(up_weight, lax.axis_index('rep') * share, share, 0)]
  transfers between devices with their start and end apart: 3 -> 0, of which waited for: 3 -> 0; matrix products, arithmetic and copies ran while one was open for 11% -> 0% of each run, Pallas kernels for 0% -> 0%
where the time goes in v1:
time: 83.9 us; the launch traced here: 83.3 us
  Pallas kernels  81.4 us (97%)
  local copies, waits for them, and re-layouts  1.88 us (2%)
    pallas_call x1, Pallas kernels, fused(): pl.pallas_call(functools.partial(kernel, n), out_shape=jax.ShapeDtypeStru...  81.4 us
    unnamed x1, local copies, waits for them, and re-layouts  1.88 us

profile of v1, /device:TPU:0, one launch (start us, length us, event | category | flops | bytes accessed | tf_op | source)
XLA Modules:
  0.0 83.3 jit_solution(8409191379220294490)
XLA Ops:
  0.0 81.4 %shard_map.46 = bf16[128,2048]{1,0:T(8,128)(2,1)} custom-call(bf16[512,2048]{1,0:T(8,128)(2,1)} %tok_hbm.1, f32[1,2048]{1,0:T(1,128)} %bitcast.1, bf16[512,1024]{1,0:T(8,128)(2,1)} %up_hbm.1, bf16[1024,512]{1,0:T(8,128)(2,1)} %dn_hbm.1), custom_call_target="tpu_custom_call" | custom-call | tf_op jit(solution)/shard_map/pallas_call | solution.py:294
  81.4 1.9 %copy.6 = bf16[128,2048]{1,0:T(8,128)(2,1)} copy(bf16[128,2048]{1,0:T(8,128)(2,1)} %shard_map.46) | data formatting | bytes 1048576

commit v2 on v1

--- a/solution.py
+++ b/solution.py
@@ -9,7 +9,8 @@
 
 EPS = 1e-06
 UP_CHUNKS = 2
-CHUNK_COLS = 256
+CHUNK_COLS = 128
+LAG = 4
 
 
 def shards(tokens, norm_gain, up_weight, down_weight):
@@ -48,8 +49,8 @@
 
 
 def kernel(
-    n, tok_hbm, gain_ref, up_hbm, dn_hbm, out_hbm,
-    tok, nrm, upw, dnw, hid, acc, keep, asend, arecv, bsend, brecv, outv,
+    n, tok_hbm, gain_hbm, up_hbm, dn_hbm, out_hbm,
+    gain_ref, tok, nrm, upw, dnw, hid, acc, keep, asend, arecv, bsend, brecv, outv,
     up_send, up_recv, dn_send, dn_recv, tok_send, tok_recv,
     a_send, a_recv, b_send, b_recv, local, out_sem,
 ):
@@ -98,7 +99,7 @@
 
     def send_own_dn(side):
         for c in range(DC):
-            dn_copy(side, z, c, dn_own(c)).start()
+            dn_copy(side, z, c, dnw.at[z * DC + c]).start()
 
     def source(p):
         m = jnp.minimum(z, n - 1 - z)
@@ -107,14 +108,6 @@
             p <= 2 * m, jnp.where(p % 2 == 1, 1, -1), jnp.where(z < n - 1 - z, 1, -1)
         )
         return z + sign * k
-
-    loads = [pltpu.make_async_copy(tok_hbm, tok.at[y], local.at[0])]
-    for c in range(UC):
-        loads.append(pltpu.make_async_copy(up_own(c), up_slot(z, c), local.at[1 + c]))
-    for c in range(DC):
-        loads.append(pltpu.make_async_copy(dn_own(c), dnw.at[z * DC + c], local.at[1 + UC + c]))
-    for load in loads:
-        load.start()
 
     peers = [at(y, z, partner)]
     for j in (1, 2, 3):
@@ -129,19 +122,33 @@
             pl.semaphore_signal(
                 barrier, inc=1, device_id=beside(side), device_id_type=pl.DeviceIdType.MESH
             )
+    up_loads = [
+        pltpu.make_async_copy(up_own(c), up_slot(z, c), local.at[c]) for c in range(UC)
+    ]
+    dn_loads = [
+        pltpu.make_async_copy(dn_own(c), dnw.at[z * DC + c], local.at[UC + c]) for c in range(DC)
+    ]
+    tok_load = pltpu.make_async_copy(tok_hbm, tok.at[y], local.at[UC + DC])
+    gain_load = pltpu.make_async_copy(gain_hbm, gain_ref, local.at[UC + DC + 1])
+    for load in up_loads + dn_loads + [gain_load, tok_load]:
+        load.start()
+
     greeted = 4 + jnp.where(has[0], 1, 0) + jnp.where(has[1], 1, 0)
     pl.semaphore_wait(barrier, greeted)
 
-    for side in (0, 1):
-        @pl.when(has[side])
-        def _():
-            for c in range(UC):
-                up_copy(side, z, c, up_own(c)).start()
+    for c in range(UC):
+        up_loads[c].wait()
+        for side in (0, 1):
+            @pl.when(has[side])
+            def _():
+                up_copy(side, z, c, up_slot(z, c)).start()
 
     part = pl.ds(pl.multiple_of(core * half, half), half)
     across = remote(tok_hbm.at[part, :], tok.at[y, part, :], tok_send.at[0], tok_recv.at[0],
                     at(1 - y, z, t))
     across.start()
+    for load in dn_loads:
+        load.wait()
 
     @pl.when(z == 0)
     def _():
@@ -151,6 +158,7 @@
     def _():
         send_own_dn(0)
 
+    gain_load.wait()
     gain = gain_ref[...]
 
     def normalise(yy):
@@ -162,7 +170,7 @@
             return carry
         lax.fori_loop(0, 4, tile, 0)
 
-    loads[0].wait()
+    tok_load.wait()
     normalise(y)
 
     for p in range(1, n):
@@ -186,8 +194,6 @@
     remote(tok.at[1 - y, theirs, :], tok.at[1 - y, theirs, :], tok_send.at[1], tok_recv.at[1],
            at(y, z, partner)).wait_recv()
     normalise(1 - y)
-    for load in loads[1:]:
-        load.wait()
 
     def lift(i, carry):
         r = pl.ds(pl.multiple_of(i * half, half), half)
@@ -242,23 +248,31 @@
         asend[i] = jnp.dot(first, block, preferred_element_type=jnp.float32).astype(jnp.bfloat16)
         a_copy(i).start()
         second = hid[pl.ds(pl.multiple_of(core * rows, rows), rows), :]
-        acc[...] = jnp.dot(second, block, preferred_element_type=jnp.float32)
+        acc[i % 2] = jnp.dot(second, block, preferred_element_type=jnp.float32)
+
+        @pl.when(i > 0)
+        def _():
+            join(i - 1)
+
+        @pl.when(i >= LAG)
+        def _():
+            finish(i - LAG)
+        return carry
+
+    def join(i):
         a_copy(i).wait_recv()
         for q in range(4):
             r = pl.ds(q * own_rows, own_rows)
-            bsend[i, q] = (acc[r, :] + arecv[i, r, :].astype(jnp.float32)).astype(jnp.bfloat16)
+            bsend[i, q] = (acc[i % 2, r, :] + arecv[i, r, :].astype(jnp.float32)).astype(jnp.bfloat16)
         for j in (3, 2, 1):
             b_copy(i, j).start()
         r = pl.ds(pl.multiple_of(own_q * own_rows, own_rows), own_rows)
-        keep[i] = acc[r, :] + arecv[i, r, :].astype(jnp.float32)
-
-        @pl.when(i > 0)
-        def _():
-            finish(i - 1)
-        return carry
+        keep[i] = acc[i % 2, r, :] + arecv[i, r, :].astype(jnp.float32)
 
     lax.fori_loop(0, total, step, 0)
-    finish(total - 1)
+    join(total - 1)
+    for i in range(total - LAG, total):
+        finish(i)
 
     across.wait_send()
     over.wait_send()
@@ -296,18 +310,19 @@
         out_shape=jax.ShapeDtypeStruct((own_rows, D), bf),
         in_specs=[
             pl.BlockSpec(memory_space=pl.ANY),
-            pl.BlockSpec(memory_space=pltpu.VMEM),
+            pl.BlockSpec(memory_space=pl.ANY),
             pl.BlockSpec(memory_space=pl.ANY),
             pl.BlockSpec(memory_space=pl.ANY),
         ],
         out_specs=pl.BlockSpec(memory_space=pl.ANY),
         scratch_shapes=[
+            pltpu.VMEM((1, D), f32),
             pltpu.VMEM((2, rows, D), bf),
             pltpu.VMEM((2 * rows, D), bf),
             pltpu.VMEM((n * up_rows, H), bf),
             pltpu.VMEM((n * DC, H, CW), bf),
             pltpu.VMEM((2 * rows, H), bf),
-            pltpu.VMEM((rows, CW), f32),
+            pltpu.VMEM((2, rows, CW), f32),
             pltpu.VMEM((total, own_rows, CW), f32),
             pltpu.VMEM((total, rows, CW), bf),
             pltpu.VMEM((total, rows, CW), bf),
@@ -324,11 +339,11 @@
             dma((total,)),
             dma((total, 3)),
             dma((total, 3)),
-            dma((1 + UP_CHUNKS + DC,)),
+            dma((2 + UP_CHUNKS + DC,)),
             dma((total,)),
         ],
         compiler_params=pltpu.CompilerParams(
-            collective_id=0, has_side_effects=True, vmem_limit_bytes=58 * 1024 * 1024
+            collective_id=0, has_side_effects=True, vmem_limit_bytes=53 * 1024 * 1024
         ),
     )(tokens, norm_gain.reshape(1, D), up_weight, down_weight)
 

time: 83.9 us -> 83 us (0.989)
    unnamed x1 -> x3, local copies, waits for them, and re-layouts: 1.88 us -> 1.49 us
where the time goes in v2:
time: 83 us; the launch traced here: 82.8 us
  Pallas kernels  81.3 us (98%)
  local copies, waits for them, and re-layouts  1.49 us (2%)
    pallas_call x1, Pallas kernels, fused(): pl.pallas_call(functools.partial(kernel, n), out_shape=jax.ShapeDtypeStru...  81.3 us

profile of v2, /device:TPU:0, one launch (start us, length us, event | category | flops | bytes accessed | tf_op | source)
XLA Modules:
  0.0 82.8 jit_solution(17489539154581936224)
XLA Ops:
  0.0 0.0 copy-start
  0.0 0.7 copy-done
  0.7 81.3 %shard_map.46 = bf16[128,2048]{1,0:T(8,128)(2,1)S(1)} custom-call(bf16[512,2048]{1,0:T(8,128)(2,1)} %tok_hbm.1, f32[1,2048]{1,0:T(1,128)S(1)} %bitcast.1, bf16[512,1024]{1,0:T(8,128)(2,1)} %up_hbm.1, bf16[1024,512]{1,0:T(8,128)(2,1)} %dn_hbm.1), custom_call_target="tpu_custom_call" | custom-call | tf_op jit(solution)/shard_map/pallas_call | solution.py:308
  82.0 0.8 copy.6
Async XLA Ops:
  0.0 0.7 copy-start

commit v3 on v2

--- a/solution.py
+++ b/solution.py
@@ -97,9 +97,23 @@
         return remote(src, dnw.at[s * DC + c], dn_send.at[side, s * DC + c],
                       dn_recv.at[s * DC + c], beside(side))
 
+    def dn_pair(side, s, c):
+        two = dnw.at[pl.ds(s * DC + c, 2)]
+        return remote(two, two, dn_send.at[side, s * DC + c], dn_recv.at[s * DC + c], beside(side))
+
+    def outer(s):
+        return (s == 0) | (s == n - 1)
+
     def send_own_dn(side):
-        for c in range(DC):
-            dn_copy(side, z, c, dnw.at[z * DC + c]).start()
+        @pl.when(outer(z))
+        def _():
+            for c in range(DC):
+                dn_copy(side, z, c, dnw.at[z * DC + c]).start()
+
+        @pl.when(jnp.logical_not(outer(z)))
+        def _():
+            for c in range(0, DC, 2):
+                dn_pair(side, z, c).start()
 
     def source(p):
         m = jnp.minimum(z, n - 1 - z)
@@ -235,13 +249,21 @@
         p, c = i // DC, i % DC
         s = source(p)
 
-        @pl.when(p > 0)
+        @pl.when((p > 0) & outer(s))
         def _():
             dn_copy(0, s, c, dnw.at[s * DC + c]).wait_recv()
             for side in (0, 1):
                 @pl.when(((s > z) if side == 0 else (s < z)) & has[side])
                 def _():
                     dn_copy(side, s, c, dnw.at[s * DC + c]).start()
+
+        @pl.when((p > 0) & jnp.logical_not(outer(s)) & (c % 2 == 0))
+        def _():
+            dn_pair(0, s, c).wait_recv()
+            for side in (0, 1):
+                @pl.when(((s > z) if side == 0 else (s < z)) & has[side])
+                def _():
+                    dn_pair(side, s, c).start()
 
         block = dnw[s * DC + c]
         first = hid[pl.ds(pl.multiple_of((1 - core) * rows, rows), rows), :]
@@ -271,11 +293,23 @@
 
     lax.fori_loop(0, total, step, 0)
     join(total - 1)
-    for i in range(total - LAG, total):
+    for i in range(total - LAG, total - 1):
         finish(i)
 
     across.wait_send()
     over.wait_send()
+    for side in (0, 1):
+        for s in range(n):
+            @pl.when(((z <= s) if side == 0 else (z >= s)) & has[side])
+            def _():
+                for c in range(UC):
+                    up_copy(side, s, c, up_slot(s, c)).wait_send()
+                if s in (0, n - 1):
+                    for c in range(DC):
+                        dn_copy(side, s, c, dnw.at[s * DC + c]).wait_send()
+                else:
+                    for c in range(0, DC, 2):
+                        dn_pair(side, s, c).wait_send()
 
     def drain(i, carry):
         a_copy(i).wait_send()
@@ -284,15 +318,9 @@
         out_copy(i).wait()
         return carry
 
-    lax.fori_loop(0, total, drain, 0)
-    for side in (0, 1):
-        for s in range(n):
-            @pl.when(((z <= s) if side == 0 else (z >= s)) & has[side])
-            def _():
-                for c in range(UC):
-                    up_copy(side, s, c, up_slot(s, c)).wait_send()
-                for c in range(DC):
-                    dn_copy(side, s, c, dnw.at[s * DC + c]).wait_send()
+    lax.fori_loop(0, total - 1, drain, 0)
+    finish(total - 1)
+    drain(total - 1, 0)
 
 
 def fused(n, tokens, norm_gain, up_weight, down_weight):
@@ -358,7 +386,7 @@
         mesh.shape["rep"] == 2
         and mesh.shape["tp"] == 4
         and n <= 8
-        and columns % CHUNK_COLS == 0
+        and columns % (2 * CHUNK_COLS) == 0
         and depth % (UP_CHUNKS * 16) == 0
         and hidden % 256 == 0
         and rows % 64 == 0

time: 83 us -> 82.8 us (level)
  no operation moved by 1% of the time
where the time goes in v3:
time: 82.8 us; the launch traced here: 82.6 us
  Pallas kernels  81.1 us (98%)
  local copies, waits for them, and re-layouts  1.49 us (2%)
    pallas_call x1, Pallas kernels, fused(): pl.pallas_call(functools.partial(kernel, n), out_shape=jax.ShapeDtypeStru...  81.1 us

profile of v3, /device:TPU:0, one launch (start us, length us, event | category | flops | bytes accessed | tf_op | source)
XLA Modules:
  0.0 82.6 jit_solution(11400334978404082824)
XLA Ops:
  0.0 0.0 copy-start
  0.0 0.7 copy-done
  0.7 81.1 %shard_map.46 = bf16[128,2048]{1,0:T(8,128)(2,1)S(1)} custom-call(bf16[512,2048]{1,0:T(8,128)(2,1)} %tok_hbm.1, f32[1,2048]{1,0:T(1,128)S(1)} %bitcast.1, bf16[512,1024]{1,0:T(8,128)(2,1)} %up_hbm.1, bf16[1024,512]{1,0:T(8,128)(2,1)} %dn_hbm.1), custom_call_target="tpu_custom_call" | custom-call | tf_op jit(solution)/shard_map/pallas_call | solution.py:336
  81.8 0.8 copy.6
Async XLA Ops:
  0.0 0.7 copy-start
